TPU v7x, 32 devices: a whole 2x2x4 slice. The times are simulated.
32 devices in a mesh: sp: 8 (over z, y), tp: 4 (over x, core).
Axes of the slice: x: 2, y: 2, z: 4, core: 2. Of those that a mesh axis runs over, the one named last changes fastest.
Arguments:
- latent: bfloat16 [4096, 4096], P(('sp', 'tp')), may hold values from -3 to 3
- context: bfloat16 [1024, 4096], P('sp'), may hold values from -6 to 6
- cond: float32 [4096], replicated, may hold values from -6 to 6
- ctx_cond: float32 [4096], replicated, may hold values from -6 to 6
- w_shift: bfloat16 [4096, 4096], P('sp', 'tp'), may hold values from -0.1875 to 0.1875
- w_scale: bfloat16 [4096, 4096], P('sp', 'tp'), may hold values from -0.09375 to 0.15478516
- w_gate: bfloat16 [4096, 4096], P('sp', 'tp'), may hold values from -0.1875 to 0.1875
- w_query: bfloat16 [4096, 2048], P(None, 'tp'), may hold values from -0.09375 to 0.09375
- key_weight: bfloat16 [4096, 1024], P(None, 'tp'), may hold values from -0.09375 to 0.09375
- value_weight: bfloat16 [4096, 1024], P(None, 'tp'), may hold values from -0.09375 to 0.09375
- w_out: bfloat16 [2048, 4096], P('tp'), may hold values from -0.125 to 0.125
- sink: float32 [16], replicated, may hold values from 4 to 8
Outputs:
- mixed: bfloat16 [4096, 4096], P(('sp', 'tp'))
All inputs are finite; a program needn't handle non-finite values.
Results may differ from a plain program's by a relative error of at most 0.035.
Values may be sent and summed in bfloat16 or wider, within the bound.
A program may use at most 64 MiB of HBM per device.

v0:
```python
import jax
import jax.numpy as jnp
from jax import lax
from jax.sharding import PartitionSpec as P

HEAD_SIZE = 128
WINDOW_SIDE = 128
GRID_WIDTH = 64


EPS = 1e-05
THETA = 10000.0
MASKED = -1e30


def with_halo(cells, sides, width):
    for axis, dim in sides:
        count = lax.axis_size(axis)
        ends = count - 1
        head = lax.slice_in_dim(cells, 0, width, axis=dim)
        tail = lax.slice_in_dim(cells, cells.shape[dim] - width, cells.shape[dim], axis=dim)
        cells = jnp.concatenate(
            [
                lax.ppermute(tail, axis, [(i, (i + 1) % count) for i in range(ends)]),
                cells,
                lax.ppermute(head, axis, [((i + 1) % count, i) for i in range(ends)]),
            ],
            axis=dim,
        )
    return cells


def layer_norm(rows):
    values = rows.astype(jnp.float32)
    mean = jnp.mean(values, axis=-1, keepdims=True)
    var = jnp.mean(jnp.square(values - mean), axis=-1, keepdims=True)
    return (values - mean) * lax.rsqrt(var + EPS)


def rotate_half(values, token_position, width):
    half = width // 2
    inverse = THETA ** (-jnp.arange(half, dtype=jnp.float32) * 2.0 / width)
    angle = token_position.astype(jnp.float32)[:, None] * inverse[None, :]
    cosine = jnp.cos(angle)[:, None, :]
    sine = jnp.sin(angle)[:, None, :]
    first = values[..., :half]
    second = values[..., half:]
    return jnp.concatenate(
        [first * cosine - second * sine, second * cosine + first * sine], axis=-1
    )


def axial_rotation(heads, token_position, grid):
    width = heads.shape[-1] // 2
    values = heads.astype(jnp.float32)
    turned = jnp.concatenate(
        [
            rotate_half(values[..., :width], token_position // grid, width),
            rotate_half(values[..., width:], token_position % grid, width),
        ],
        axis=-1,
    )
    return turned.astype(jnp.bfloat16)


def sink_weights(scores, sink_column):
    top = jnp.maximum(jnp.max(scores, axis=-1, keepdims=True), sink_column)
    expo = jnp.exp(scores - top)
    return (expo / (jnp.sum(expo, axis=-1, keepdims=True) + jnp.exp(sink_column - top))).astype(
        jnp.bfloat16
    )


def shards(
    latent,
    context,
    cond,
    ctx_cond,
    w_shift,
    w_scale,
    w_gate,
    w_query,
    key_weight,
    value_weight,
    w_out,
    sink,
):
    sp_count = lax.axis_size("sp")
    sp_index = lax.axis_index("sp")
    tp_index = lax.axis_index("tp")
    block_rows = w_shift.shape[0]
    act = jax.nn.silu(jnp.stack([cond, ctx_cond])).astype(jnp.bfloat16)
    own_act = lax.dynamic_slice_in_dim(act, sp_index * block_rows, block_rows, 1)
    shift_part = jnp.dot(own_act, w_shift, preferred_element_type=jnp.float32)
    scale_part = jnp.dot(own_act, w_scale, preferred_element_type=jnp.float32)
    gate_part = jnp.dot(own_act[0:1], w_gate, preferred_element_type=jnp.float32)
    shift_sum, scale_sum, gate_sum = lax.psum((shift_part, scale_part, gate_part), "sp")
    shift, scale, gate = (
        lax.all_gather(shift_sum, "tp", axis=1, tiled=True),
        lax.all_gather(scale_sum, "tp", axis=1, tiled=True),
        lax.all_gather(gate_sum, "tp", axis=1, tiled=True),
    )
    latent_mod = (layer_norm(latent) * (1.0 + scale[0]) + shift[0]).astype(jnp.bfloat16)
    ctx_mod = (layer_norm(context) * (1.0 + scale[1]) + shift[1]).astype(jnp.bfloat16)
    kv_cols = key_weight.shape[1]
    q_cols = w_query.shape[1]
    ctx_pair = lax.all_gather(
        jnp.concatenate(
            [
                jnp.dot(ctx_mod, key_weight, preferred_element_type=jnp.float32).astype(
                    jnp.bfloat16
                ),
                jnp.dot(ctx_mod, value_weight, preferred_element_type=jnp.float32).astype(
                    jnp.bfloat16
                ),
            ],
            axis=1,
        ),
        "sp",
        axis=0,
        tiled=True,
    )
    piece = lax.all_gather(latent_mod, "tp", axis=0, tiled=True)
    projected_rows = jnp.concatenate(
        [
            jnp.dot(piece, w_query, preferred_element_type=jnp.float32).astype(jnp.bfloat16),
            jnp.dot(piece, key_weight, preferred_element_type=jnp.float32).astype(jnp.bfloat16),
            jnp.dot(piece, value_weight, preferred_element_type=jnp.float32).astype(jnp.bfloat16),
        ],
        axis=1,
    )
    tokens_here = projected_rows.shape[0]
    kv_heads = kv_cols // HEAD_SIZE
    q_heads = q_cols // HEAD_SIZE
    query_group = q_heads // kv_heads
    offset = sp_index * tokens_here
    token_position = offset + jnp.arange(tokens_here, dtype=jnp.int32)
    query = axial_rotation(
        projected_rows[:, :q_cols].reshape(tokens_here, q_heads, HEAD_SIZE),
        token_position,
        GRID_WIDTH,
    )
    key = axial_rotation(
        projected_rows[:, q_cols : q_cols + kv_cols].reshape(tokens_here, kv_heads, HEAD_SIZE),
        token_position,
        GRID_WIDTH,
    )
    value_rows = projected_rows[:, q_cols + kv_cols :]
    extended = with_halo(
        jnp.concatenate([key.reshape(tokens_here, kv_cols), value_rows], axis=1),
        (("sp", 0),),
        WINDOW_SIDE,
    )
    block_list = tokens_here // WINDOW_SIDE
    band = jnp.concatenate(
        [
            extended[shift_index * WINDOW_SIDE : shift_index * WINDOW_SIDE + tokens_here].reshape(
                block_list, WINDOW_SIDE, 2 * kv_cols
            )
            for shift_index in range(3)
        ],
        axis=1,
    )
    band_key = band[..., :kv_cols].reshape(block_list, 3 * WINDOW_SIDE, kv_heads, HEAD_SIZE)
    band_value = band[..., kv_cols:].reshape(block_list, 3 * WINDOW_SIDE, kv_heads, HEAD_SIZE)
    context_key_rows = ctx_pair[:, :kv_cols].reshape(-1, kv_heads, HEAD_SIZE)
    context_value_rows = ctx_pair[:, kv_cols:].reshape(-1, kv_heads, HEAD_SIZE)
    query_block_list = query.reshape(block_list, WINDOW_SIDE, kv_heads, query_group, HEAD_SIZE)
    factor = HEAD_SIZE ** (-0.5)
    band_scores = (
        jnp.einsum(
            "nqhgd,nkhd->nhgqk", query_block_list, band_key, preferred_element_type=jnp.float32
        )
        * factor
    )
    total = tokens_here * sp_count
    qpos = token_position.reshape(block_list, WINDOW_SIDE)[:, :, None]
    kpos = (
        offset
        - WINDOW_SIDE
        + (jnp.arange(block_list, dtype=jnp.int32) * WINDOW_SIDE)[:, None, None]
        + jnp.arange(3 * WINDOW_SIDE, dtype=jnp.int32)[None, None, :]
    )
    valid = (jnp.abs(kpos - qpos) <= WINDOW_SIDE) & (kpos >= 0) & (kpos < total)
    band_scores = jnp.where(valid[:, None, None], band_scores, MASKED)
    ctx_scores = (
        jnp.einsum(
            "nqhgd,khd->nhgqk",
            query_block_list,
            context_key_rows,
            preferred_element_type=jnp.float32,
        )
        * factor
    )
    own_sink = lax.dynamic_slice_in_dim(sink, tp_index * q_heads, q_heads).reshape(
        kv_heads, query_group
    )[:, :, None, None]
    weights = sink_weights(jnp.concatenate([band_scores, ctx_scores], axis=-1), own_sink)
    attended = jnp.einsum(
        "nhgqk,nkhd->nqhgd",
        weights[..., : 3 * WINDOW_SIDE],
        band_value,
        preferred_element_type=jnp.float32,
    ) + jnp.einsum(
        "nhgqk,khd->nqhgd",
        weights[..., 3 * WINDOW_SIDE :],
        context_value_rows,
        preferred_element_type=jnp.float32,
    )
    attended = attended.astype(jnp.bfloat16).reshape(tokens_here, q_cols)
    projected = lax.psum_scatter(
        jnp.dot(attended, w_out, preferred_element_type=jnp.float32).astype(jnp.bfloat16),
        "tp",
        scatter_dimension=0,
        tiled=True,
    ).astype(jnp.float32)
    return (latent.astype(jnp.float32) + gate[0][None, :] * projected).astype(jnp.bfloat16)


def solution(mesh):
    in_specs = (
        P(("sp", "tp"), None),
        P("sp", None),
        P(),
        P(),
        P("sp", "tp"),
        P("sp", "tp"),
        P("sp", "tp"),
        P(None, "tp"),
        P(None, "tp"),
        P(None, "tp"),
        P("tp", None),
        P(),
    )
    out_specs = P(("sp", "tp"), None)
    return jax.shard_map(shards, mesh=mesh, in_specs=in_specs, out_specs=out_specs, check_vma=False)
```

profile of v0, /device:TPU:14, one launch (start us, length us, event | category | flops | bytes accessed | tf_op | source)
XLA Modules:
  0.0 256.4 jit_solution(11385487950224661711)
XLA Ops:
  6.5 0.9 fusion.39
  7.5 1.5 fusion.55
  9.0 1.5 fusion.54
  10.5 1.5 fusion.42
  11.9 30.1 %all-reduce = (f32[2,1024]{1,0:T(2,128)S(1)}, f32[2,1024]{1,0:T(2,128)S(1)}, f32[1,1024]{1,0:T(1,128)S(1)}) all-reduce(f32[2,1024]{1,0:T(2,128)S(1)} %fusion.55, f32[2,1024]{1,0:T(2,128)S(1)} %fusion.54, f32[1,1024]{1,0:T(1,128)S(1)} %fusion.42), channel_id=1, replica_groups=mesh['sp'=8,'tp'=4] {'sp'}, use_global_device_ids=true, to_apply=%region_4.5 | all-reduce | flops 5120 | bytes 40960 | tf_op jit(solution)/shard_map/psum | solution.py:97
  42.1 5.2 %all_gather.17 = f32[2,4096]{1,0:T(2,128)S(1)} all-gather(f32[2,1024]{1,0:T(2,128)S(1)} %get-tuple-element.5), channel_id=1, replica_groups=mesh['sp'=8,'tp'=4] {'tp'}, dimensions={1}, use_global_device_ids=true | all-gather | bytes 40960 | tf_op jit(solution)/shard_map/all_gather | solution.py:99
  47.3 5.2 %all_gather.16 = f32[2,4096]{1,0:T(2,128)S(1)} all-gather(f32[2,1024]{1,0:T(2,128)S(1)} %get-tuple-element.6), channel_id=1, replica_groups=mesh['sp'=8,'tp'=4] {'tp'}, dimensions={1}, use_global_device_ids=true | all-gather | bytes 40960 | tf_op jit(solution)/shard_map/all_gather | solution.py:100
  52.5 0.2 convert_reduce_fusion.1
  52.7 0.4 fusion.12
  53.2 2.2 convolution_convert_fusion.4
  55.4 0.6 convolution_convert_fusion.5
  56.0 0.7 pad_maximum_fusion.8
  56.7 0.2 convert_reduce_fusion
  57.0 0.4 fusion.8
  57.4 1.5 fusion.11
  58.9 0.2 reduce-scatter.2.cloned.1.call-start
  59.1 0.5 multiply_cosine_fusion.1
  59.7 0.8 copy.119
  60.5 0.8 copy.117
  61.5 0.8 copy.113
  62.7 1.9 fusion.32
  64.6 34.8 %all-gather.5.cloned.1.call-done = bf16[1024,512]{1,0:T(8,128)(2,1)} async-done(((bf16[128,512]{1,0:T(8,128)(2,1)}), bf16[1024,512]{1,0:T(8,128)(2,1)}) %all-gather.5.cloned.1.call-update) | async-done | bytes 1048592 | tf_op jit(solution)/shard_map/all_gather | solution.py:107
  99.4 2.3 fusion.49
  101.6 2.0 copy.150
  103.7 2.0 reshape.310
  105.6 29.7 %all-gather.3.cloned.1.call-done = bf16[512,4096]{1,0:T(8,128)(2,1)} async-done(((bf16[128,4096]{1,0:T(8,128)(2,1)}), bf16[512,4096]{1,0:T(8,128)(2,1)}) %all-gather.3.cloned.1.call-update) | async-done | bytes 4194320 | tf_op jit(solution)/shard_map/all_gather | solution.py:123
  135.3 5.9 %convolution_convert_fusion.1 = bf16[512,512]{0,1:T(8,128)(2,1)S(1)} fusion(bf16[512,4096]{1,0:T(8,128)(2,1)} %all-gather.3.cloned.1.call-done, bf16[4096,512]{1,0:T(8,128)(2,1)} %param.19), kind=kOutput, calls=%fused_computation.33 | convolution fusion | flops 2147745792 | bytes 8912896 | tf_op jit(solution)/shard_map/dot_general | solution.py:126
  141.3 1.0 subtract_convert_fusion.1
  142.3 0.9 concatenate.50
  143.2 1.0 copy.125
  144.2 0.9 concatenate.49
  145.2 1.0 copy.124
  146.2 0.9 concatenate.48
  147.2 1.0 copy.123
  148.2 0.9 concatenate.47
  149.1 1.1 copy.122
  150.2 3.5 %convolution_convert_fusion.3 = bf16[512,256]{0,1:T(8,128)(2,1)S(1)} fusion(bf16[512,4096]{1,0:T(8,128)(2,1)} %all-gather.3.cloned.1.call-done, bf16[4096,256]{1,0:T(8,128)(2,1)S(1)} %copy-done), kind=kOutput, calls=%fused_computation.36 | convolution fusion | flops 1073872896 | bytes 6553600 | tf_op jit(solution)/shard_map/dot_general | solution.py:127
  153.7 0.2 copy.155
  154.0 0.2 copy.154
  154.2 0.2 copy.153
  154.5 0.2 copy.152
  154.7 1.7 multiply_subtract_fusion
  156.4 1.5 multiply_subtract_fusion.1
  157.9 1.6 maximum_convert_fusion
  159.7 3.0 %convolution_convert_fusion.2 = bf16[512,256]{1,0:T(8,128)(2,1)S(1)} fusion(bf16[512,4096]{1,0:T(8,128)(2,1)S(1)} %copy-done.17, bf16[4096,256]{1,0:T(8,128)(2,1)} %param.21), kind=kOutput, calls=%fused_computation.35 | convolution fusion | flops 1073872896 | bytes 6553600 | tf_op jit(solution)/shard_map/dot_general | solution.py:128
  162.7 3.5 %collective-permute-start = (bf16[128,512]{1,0:T(8,128)(2,1)S(1)}, bf16[128,512]{1,0:T(8,128)(2,1)S(1)}, u32[]{:S(2)}, u32[]{:S(2)}) collective-permute-start(bf16[128,512]{1,0:T(8,128)(2,1)S(1)} %get-tuple-element.24), channel_id=1, source_target_pairs={{0,4},{4,8},{8,12},{12,16},{16,20},{20,24},{24,28},{1,5},{5,9},{9,... | collective-permute-start | bytes 393224 | tf_op jit(solution)/shard_map/ppermute | solution.py:24
  166.2 2.7 %collective-permute-start.1 = (bf16[128,512]{1,0:T(8,128)(2,1)S(1)}, bf16[128,512]{1,0:T(8,128)(2,1)}, u32[]{:S(2)}, u32[]{:S(2)}) collective-permute-start(bf16[128,512]{1,0:T(8,128)(2,1)S(1)} %get-tuple-element.25), channel_id=1, source_target_pairs={{4,0},{8,4},{12,8},{16,12},{20,16},{24,20},{28,24},{5,1},{9,5},{13... | collective-permute-start | bytes 393224 | tf_op jit(solution)/shard_map/ppermute | solution.py:26
  169.0 0.7 pad_maximum_fusion.5
  169.7 4.5 %fusion.52 = (f32[4,2,2,128]{3,2,0,1:T(2,128)S(1)}, f32[4,2,2,128,1024]{3,4,2,0,1:T(8,128)}) fusion(bf16[4,128,2,2,128]{4,1,3,2,0:T(8,128)(2,1)S(1)} %pad_maximum_fusion.5, bf16[1024,2,128,1,1]{2,1,0,4,3:T(2,128)(2,1)S(1)} %bitcast.86), kind=kOutput, calls=%fused_computation.104 | convolution fusion | flops 541063168 | bytes 9445376 | tf_op jit(solution)/shard_map/nqhgd,khd->nhgqk/dot_general | solution.py:187
  174.5 1.0 pad_maximum_fusion.3
  175.6 1.3 fusion.48
  176.9 1.5 copy.121
  178.4 0.7 fusion.53
  179.2 6.0 %fusion.1 = f32[4,2,2,128]{3,2,0,1:T(2,128)S(1)} fusion(f32[4,2,2,128,1024]{3,4,2,0,1:T(8,128)} %get-tuple-element.43, f32[4,2,2,128]{3,2,0,1:T(2,128)S(1)} %copy.132, f32[4,2,2,128,384]{3,4,2,1,0:T(8,128)S(1)} %get-tuple-element.45), kind=kLoop, calls=%fused_computation.4 | loop fusion | flops 8648704 | bytes 11550720 | tf_op jit(solution)/shard_map/reduce_sum | solution.py:69
  185.4 4.6 %divide_convert_fusion = bf16[4,2,2,128,1408]{3,4,2,0,1:T(8,128)(2,1)} fusion(f32[4,2,2,128,1024]{3,4,2,0,1:T(8,128)S(1)} %bitcast.78, f32[4,2,2,128]{3,2,0,1:T(2,128)S(1)} %copy.134, f32[4,2,2,128]{3,2,0,1:T(2,128)S(1)} %copy.132, f32[4,2,2,128,384]{3,4,2,1,0:T(8,128)S(1)} %get-tuple-element.45), kind=kLoop, calls=%fused_computation.2 | loop fusion | flops 11534336 | bytes 17317888 | tf_op jit(solution)/shard_map/convert_element_type | solution.py:69
  190.1 0.4 copy.120
  190.4 2.9 %fusion.22 = f32[4,128,2,2,128]{1,4,3,2,0:T(8,128)S(1)} fusion(bf16[1024,2,128,1,1]{0,2,4,1,3:T(8,128)(2,1)S(1)} %bitcast.90, bf16[4,2,2,128,1408]{3,4,2,0,1:T(8,128)(2,1)} %divide_convert_fusion), kind=kOutput, calls=%fused_computation.31 | convolution fusion | flops 536870912 | bytes 5767168 | tf_op jit(solution)/shard_map/nhgqk,khd->nqhgd/dot_general | solution.py:204
  193.4 1.9 fusion.28
  195.3 0.4 copy.138
  195.7 0.2 reshape.312
  195.9 6.5 %convolution_convert_fusion = bf16[512,4096]{1,0:T(8,128)(2,1)} fusion(bf16[512,512]{1,0:T(8,128)(2,1)S(1)} %reshape.312, bf16[512,4096]{1,0:T(8,128)(2,1)} %param.22), kind=kOutput, calls=%fused_computation.5 | convolution fusion | flops 2149580800 | bytes 8912896 | tf_op jit(solution)/shard_map/dot_general | solution.py:212
  202.4 5.3 %all_gather.15 = f32[1,4096]{1,0:T(1,128)S(1)} all-gather(f32[1,1024]{1,0:T(1,128)S(1)} %get-tuple-element.7), channel_id=1, replica_groups=mesh['sp'=8,'tp'=4] {'tp'}, dimensions={1}, use_global_device_ids=true | all-gather | bytes 20480 | tf_op jit(solution)/shard_map/all_gather | solution.py:101
  207.7 39.7 %reduce-scatter.2.cloned.1.call-done = bf16[128,4096]{1,0:T(8,128)(2,1)} async-done(((bf16[512,4096]{1,0:T(8,128)(2,1)}), bf16[128,4096]{1,0:T(8,128)(2,1)}) %reduce-scatter.2.cloned.1.call-update) | async-done | bytes 1048592 | tf_op jit(solution)/shard_map/reduce_scatter | solution.py:211
  247.4 2.5 fusion.16
  (75 shorter events, 1.5 us)
Async XLA Ops:
  6.5 48.8 %copy-start = (bf16[4096,256]{1,0:T(8,128)(2,1)S(1)}, bf16[4096,256]{1,0:T(8,128)(2,1)}, u32[]{:S(2)}) copy-start(bf16[4096,256]{1,0:T(8,128)(2,1)} %param.20) | copy-start | bytes 6291460
  6.5 46.0 %copy-start.3 = (bf16[128,4096]{1,0:T(8,128)(2,1)S(1)}, bf16[128,4096]{1,0:T(8,128)(2,1)}, u32[]{:S(2)}) copy-start(bf16[128,4096]{1,0:T(8,128)(2,1)} %param.13) | copy-start | bytes 3145732
  6.5 92.8 %all-gather.5.cloned.1.call-start = ((), (), s32[]{:S(2)}) async-start(), calls=%async_computation.2 | async-start | bytes 1179648 | tf_op jit(solution)/shard_map/all_gather | solution.py:107
  52.7 2.6 %copy-start.4 = (bf16[128,4096]{1,0:T(8,128)(2,1)S(1)}, bf16[128,4096]{1,0:T(8,128)(2,1)}, u32[]{:S(2)}) copy-start(bf16[128,4096]{1,0:T(8,128)(2,1)} %param.13) | copy-start | bytes 3145732
  55.4 1.3 copy-start.2
  56.7 78.6 %all-gather.3.cloned.1.call-start = ((), (), s32[]{:S(2)}) async-start(), calls=%async_computation.1 | async-start | bytes 5242880 | tf_op jit(solution)/shard_map/all_gather | solution.py:123
  56.9 5.4 %copy-start.18 = (f32[16]{0:T(128)S(1)}, f32[16]{0:T(128)}, u32[]{:S(2)}) copy-start(f32[16]{0:T(128)} %param.23) | copy-start | bytes 196
  58.9 188.5 %reduce-scatter.2.cloned.1.call-start = ((), (), s32[]{:S(2)}) async-start(), calls=%async_computation.3 | async-start | bytes 5242880 | tf_op jit(solution)/shard_map/reduce_scatter | solution.py:211
  59.7 1.7 copy-start.12
  59.7 1.7 copy-start.14
  135.3 6.0 %copy-start.13 = (f32[512,32]{0,1:T(8,128)S(1)}, f32[512,32]{0,1:T(8,128)}, u32[]{:S(2)}) copy-start(f32[512,32]{0,1:T(8,128)} %copy-done.12) | copy-start | bytes 196612
  135.3 6.0 %copy-start.15 = (f32[512,32]{0,1:T(8,128)S(1)}, f32[512,32]{0,1:T(8,128)}, u32[]{:S(2)}) copy-start(f32[512,32]{0,1:T(8,128)} %copy-done.14) | copy-start | bytes 196612
  154.7 4.9 %copy-start.17 = (bf16[512,4096]{1,0:T(8,128)(2,1)S(1)}, bf16[512,4096]{1,0:T(8,128)(2,1)}, u32[]{:S(2)}) copy-start(bf16[512,4096]{1,0:T(8,128)(2,1)} %all-gather.3.cloned.1.call-done) | copy-start | bytes 12582916
  159.6 9.3 %copy-start.6 = (bf16[4,128,2,2,32]{4,1,3,2,0:T(8,128)(2,1)S(1)}, bf16[4,128,2,2,32]{4,1,3,2,0:T(8,128)(2,1)}, u32[]{:S(2)}) copy-start(bf16[4,128,2,2,32]{4,1,3,2,0:T(8,128)(2,1)} %copy.125) | copy-start | bytes 393220
  159.6 9.3 %copy-start.7 = (bf16[4,128,2,2,32]{4,1,3,2,0:T(8,128)(2,1)S(1)}, bf16[4,128,2,2,32]{4,1,3,2,0:T(8,128)(2,1)}, u32[]{:S(2)}) copy-start(bf16[4,128,2,2,32]{4,1,3,2,0:T(8,128)(2,1)} %copy.124) | copy-start | bytes 393220
  159.6 9.3 %copy-start.8 = (bf16[4,128,2,2,32]{4,1,3,2,0:T(8,128)(2,1)S(1)}, bf16[4,128,2,2,32]{4,1,3,2,0:T(8,128)(2,1)}, u32[]{:S(2)}) copy-start(bf16[4,128,2,2,32]{4,1,3,2,0:T(8,128)(2,1)} %copy.123) | copy-start | bytes 393220
  159.6 9.3 %copy-start.9 = (bf16[4,128,2,2,32]{4,1,3,2,0:T(8,128)(2,1)S(1)}, bf16[4,128,2,2,32]{4,1,3,2,0:T(8,128)(2,1)}, u32[]{:S(2)}) copy-start(bf16[4,128,2,2,32]{4,1,3,2,0:T(8,128)(2,1)} %copy.122) | copy-start | bytes 393220
  162.7 7.0 %copy-start.10 = (bf16[1024,2,128]{2,1,0:T(2,128)(2,1)S(1)}, bf16[1024,2,128]{2,1,0:T(2,128)(2,1)}, u32[]{:S(2)}) copy-start(bf16[1024,2,128]{2,1,0:T(2,128)(2,1)} %reshape.310) | copy-start | bytes 1572868
  162.7 11.6 %collective-permute-start = (bf16[128,512]{1,0:T(8,128)(2,1)S(1)}, bf16[128,512]{1,0:T(8,128)(2,1)S(1)}, u32[]{:S(2)}, u32[]{:S(2)}) collective-permute-start(bf16[128,512]{1,0:T(8,128)(2,1)S(1)} %get-tuple-element.24), channel_id=1, source_target_pairs={{0,4},{4,8},{8,12},{12,16},{16,20},{20,24},{24,28},{1,5},{5,9},{9,... | collective-permute-start | bytes 393224 | tf_op jit(solution)/shard_map/ppermute | solution.py:24
  166.2 8.3 %collective-permute-start.1 = (bf16[128,512]{1,0:T(8,128)(2,1)S(1)}, bf16[128,512]{1,0:T(8,128)(2,1)}, u32[]{:S(2)}, u32[]{:S(2)}) collective-permute-start(bf16[128,512]{1,0:T(8,128)(2,1)S(1)} %get-tuple-element.25), channel_id=1, source_target_pairs={{4,0},{8,4},{12,8},{16,12},{20,16},{24,20},{28,24},{5,1},{9,5},{13... | collective-permute-start | bytes 393224 | tf_op jit(solution)/shard_map/ppermute | solution.py:26
  175.6 2.8 %copy-start.11 = (pred[4,128,384]{1,2,0:T(8,128)(4,1)S(1)}, pred[4,128,384]{1,2,0:T(8,128)(4,1)}, u32[]{:S(2)}) copy-start(pred[4,128,384]{1,2,0:T(8,128)(4,1)} %fusion.32) | copy-start | bytes 589828
  178.4 6.9 %slice-start = ((s8[8388608]{0:T(1024)(128)(4,1)}), s8[4194304]{0:T(1024)(128)(4,1)S(1)}, s32[]{:S(2)}) async-start(s8[8388608]{0:T(1024)(128)(4,1)} %bitcast.77), calls=%async_computation.4 | async-start | bytes 8388608
  179.2 6.1 %slice-start.1 = ((s8[8388608]{0:T(1024)(128)(4,1)}), s8[4194304]{0:T(1024)(128)(4,1)S(1)}, s32[]{:S(2)}) async-start(s8[8388608]{0:T(1024)(128)(4,1)} %bitcast.77), calls=%async_computation.5 | async-start | bytes 8388608
  185.4 4.7 %copy-start.5 = (bf16[4,384,256]{2,1,0:T(8,128)(2,1)S(1)}, bf16[4,384,256]{2,1,0:T(8,128)(2,1)}, u32[]{:S(2)}) copy-start(bf16[4,384,256]{2,1,0:T(8,128)(2,1)} %get-tuple-element.8) | copy-start | bytes 2359300
  185.4 5.0 %copy-start.16 = (bf16[1024,256]{0,1:T(8,128)(2,1)S(1)}, bf16[1024,256]{0,1:T(8,128)(2,1)}, u32[]{:S(2)}) copy-start(bf16[1024,256]{0,1:T(8,128)(2,1)} %copy.150) | copy-start | bytes 1572868
  202.4 47.5 %copy-start.1 = (bf16[4096,256]{1,0:T(8,128)(2,1)S(1)}, bf16[4096,256]{1,0:T(8,128)(2,1)}, u32[]{:S(2)}) copy-start(bf16[4096,256]{1,0:T(8,128)(2,1)} %param.20) | copy-start | bytes 6291460
Sparse Core Ops, SparseCore 0:
  56.8 42.5 all-gather.4
  100.9 34.3 all-gather.2
  202.5 44.8 reduce-scatter.1
where the time goes:
time: 260 us; the launch traced here: 256 us
  waiting for transfers between devices  104 us (40%)
  blocking collectives  45.8 us (18%)
  matrix products  36.1 us (14%)
  other arithmetic  28.1 us (11%)
  local copies, waits for them, and re-layouts  22.1 us (8%)
  between operations  13.6 us (5%)
  starting transfers between devices  6.46 us (2%)
    reduce_scatter x1, waiting for transfers between devices, shards(): lax.psum_scatter(jnp.dot(attended, w_out, preferred_element_type=jnp.floa...  39.7 us
    all_gather x1, waiting for transfers between devices, shards(): lax.all_gather(jnp.concatenate([jnp.dot(ctx_mod, key_weight, preferred_el...  34.8 us
    psum x1, blocking collectives, shards(): lax.psum((shift_part, scale_part, gate_part), 'sp')  30.1 us
    all_gather x1, waiting for transfers between devices, shards(): piece = lax.all_gather(latent_mod, 'tp', axis=0, tiled=True)  29.7 us
    concatenate x8, local copies, waits for them, and re-layouts, axial_rotation(): jnp.concatenate([rotate_half(values[..., :width], token_position // grid,...  7.91 us
    dot_general x1, matrix products, shards(): jnp.dot(attended, w_out, preferred_element_type=jnp.float32)  6.47 us
    reduce_sum x1, other arithmetic, sink_weights(): jnp.sum(expo, axis=-1, keepdims=True) + jnp.exp(sink_column - top)  6.03 us
    dot_general x1, matrix products, shards(): jnp.dot(piece, w_query, preferred_element_type=jnp.float32)  5.86 us
  transfers between devices with their start and end apart: 5, of which 4 were waited for; matrix products, arithmetic and copies ran while one was open for 7% of the time, Pallas kernels for 0%

commit v1 on v0

v1 whole, which is shorter than its diff:
```python
import functools
import math

import jax
import jax.numpy as jnp
from jax import lax
from jax.experimental import pallas as pl
from jax.experimental.pallas import tpu as pltpu
from jax.sharding import PartitionSpec as P

HEAD = 128
SIDE = 128
GRID_WIDTH = 64
EPS = 1e-05
THETA = 10000.0
MASKED = -1e30
LOG2E = math.log2(math.e)
MESH = pl.DeviceIdType.MESH
F32 = jnp.float32
BF16 = jnp.bfloat16
CUTS = 2
PIECES = 4
CORES = 2


def body(
    nsp, ntp,
    lat, ctx, cond, ctx_cond, w_shift, w_scale, w_gate, w_q, w_k, w_v, w_o, sink, cos_t, sin_t,
    out,
    wmod, wq, wk, wv, wo, latb, ctxb, mb, part, mgath, tot, mod, ctxkv, q_s, kv, att,
    stage, prcv, comb, xrcv,
    load_sem, msend, mrecv, tsend, trecv, lsend, lrecv, fsend, frecv, psend, precv,
    csend, crecv, hsend, hrecv, dsend, drecv, xsend, xrecv,
):
    nx = ntp // CORES
    sp = lax.axis_index("sp")
    tp = lax.axis_index("tp")
    x = lax.div(tp, CORES)
    c = lax.rem(tp, CORES)
    oc = 1 - c
    rows, width = lat.shape
    crows = ctx.shape[0]
    cut = rows // CUTS
    tokens = rows * ntp
    mcols = w_shift.shape[1]
    qc = w_q.shape[1]
    kc = w_k.shape[1]
    kv_heads = kc // HEAD
    group = qc // kc

    def at_tp(t):
        return (sp, t)

    def at_sp(s):
        return (s, tp)

    partner = at_tp(x * CORES + oc)

    def remote(src, dst, ss, rs, dev):
        return pltpu.make_async_remote_copy(
            src_ref=src, dst_ref=dst, send_sem=ss, recv_sem=rs, device_id=dev, device_id_type=MESH
        )

    loads = [
        pltpu.make_async_copy(s, d, load_sem.at[i])
        for i, (s, d) in enumerate(
            [
                (w_shift, wmod.at[0]), (w_scale, wmod.at[1]), (w_gate, wmod.at[2]),
                (ctx, ctxb), (w_k, wk), (w_v, wv), (w_q, wq),
                (lat, latb.at[tp]), (w_o, wo),
            ]
        )
    ]
    for load in loads:
        load.start()

    barrier = pltpu.get_barrier_semaphore()
    for d in range(1, nsp):
        pl.semaphore_signal(barrier, inc=1, device_id=at_sp(lax.rem(sp + d, nsp)), device_id_type=MESH)
    for d in range(1, ntp):
        pl.semaphore_signal(barrier, inc=1, device_id=at_tp(lax.rem(tp + d, ntp)), device_id_type=MESH)
    pl.semaphore_wait(barrier, nsp + ntp - 2)

    def lat_copy(d, j):
        dst = lax.rem(x + d, nx) * CORES + c
        return remote(
            lat.at[pl.ds(j * cut, cut)], latb.at[tp, pl.ds(j * cut, cut)],
            lsend.at[d - 1, j], lrecv.at[d - 1, j], at_tp(dst),
        )

    def from_x(d):
        return lax.rem(x - d + nx, nx)

    def fwd_copy(d, j):
        slot = latb.at[from_x(d) * CORES + c, pl.ds(j * cut, cut)]
        return remote(slot, slot, fsend.at[d - 1, j], frecv.at[d - 1, j], partner)

    for d in range(1, nx):
        lat_copy(d, 0).start()
    own = remote(lat, latb.at[tp], psend, precv, partner)
    own.start()

    a0 = jax.nn.silu(cond[pl.ds(sp, 1), :]).astype(BF16).astype(F32)
    a1 = jax.nn.silu(ctx_cond[pl.ds(sp, 1), :]).astype(BF16).astype(F32)
    line = lax.broadcasted_iota(jnp.int32, (8, a0.shape[1]), 0)
    z = jnp.zeros((8, a0.shape[1]), F32)
    a0 = jnp.broadcast_to(a0, z.shape)
    a1 = jnp.broadcast_to(a1, z.shape)
    acc = None
    for i, (r0, r1) in enumerate(((0, 1), (2, 3), (4, -1))):
        act = jnp.where(line == r0, a0, jnp.where(line == r1, a1, z)).astype(BF16)
        loads[i].wait()
        piece = jnp.dot(act, wmod[i], preferred_element_type=F32)
        acc = piece if acc is None else acc + piece
    part[...] = acc
    mcopies = [
        remote(part, mgath.at[d - 1], msend.at[d - 1], mrecv.at[d - 1], at_sp(lax.rem(sp + d, nsp)))
        for d in range(1, nsp)
    ]
    for cp in mcopies:
        cp.start()
    for i in range(3, 8):
        loads[i].wait()
    acc = part[...]
    for d in range(1, nsp):
        mcopies[d - 1].wait_recv()
        acc = acc + mgath[d - 1]
    tot[...] = acc
    mine = pl.ds(pl.multiple_of(tp * mcols, mcols), mcols)
    tcopies = [
        remote(tot, mod.at[:, mine], tsend.at[d - 1], trecv.at[d - 1], at_tp(lax.rem(tp + d, ntp)))
        for d in range(1, ntp)
    ]
    for cp in tcopies:
        cp.start()
    for d in range(1, nx):
        for j in range(1, CUTS):
            lat_copy(d, j).start()
    mod[:, mine] = acc
    for cp in tcopies:
        cp.wait_recv()

    def normed(src, row0, dst, dst0, count, r_shift, r_scale):
        step = 16

        @pl.loop(0, count // step)
        def _(i):
            v = src[pl.ds(row0 + i * step, step), :].astype(F32)
            mean = jnp.mean(v, axis=-1, keepdims=True)
            v = v - mean
            var = jnp.mean(v * v, axis=-1, keepdims=True)
            v = v * lax.rsqrt(var + EPS)
            v = v * (1.0 + mod[r_scale : r_scale + 1, :]) + mod[r_shift : r_shift + 1, :]
            dst[pl.ds(dst0 + i * step, step), :] = v.astype(BF16)

    normed(ctxb, 0, mb, 0, crows, 1, 3)
    crow = pl.ds(pl.multiple_of(sp * crows, crows), crows)
    cm = mb[0:crows, :]
    ctxkv[crow, 0:kc] = jnp.dot(cm, wk[...], preferred_element_type=F32).astype(BF16)
    ctxkv[crow, kc : 2 * kc] = jnp.dot(cm, wv[...], preferred_element_type=F32).astype(BF16)
    ccopies = [
        remote(ctxkv.at[crow], ctxkv.at[crow], csend.at[d - 1], crecv.at[d - 1], at_sp(lax.rem(sp + d, nsp)))
        for d in range(1, nsp)
    ]
    for cp in ccopies:
        cp.start()

    for d in range(1, nx):
        lat_copy(d, 0).wait_recv()
        fwd_copy(d, 0).start()

    lane = lax.broadcasted_iota(jnp.int32, (1, HEAD), 1)
    low = lax.rem(lane, HEAD // 2) < HEAD // 4

    def turn(v, row0, count, factor):
        v = v.astype(BF16).astype(F32)
        swapped = jnp.where(low, pltpu.roll(v, HEAD - HEAD // 4, 1), pltpu.roll(v, HEAD // 4, 1))
        r = v * cos_t[pl.ds(row0, count), :] + swapped * sin_t[pl.ds(row0, count), :]
        return (r * factor).astype(BF16)

    def project(segments):
        total = sum(n for _, n in segments)
        qf = HEAD ** (-0.5) * LOG2E
        for w, cols, kind in ((wq, qc, 0), (wk, kc, 1), (wv, kc, 2)):
            tile = min(256, cols)
            for n0 in range(0, cols, tile):
                r = jnp.dot(mb[0:total, :], w[:, n0 : n0 + tile], preferred_element_type=F32)
                off = 0
                for row0, n in segments:
                    for h in range(0, tile, HEAD):
                        v = r[off : off + n, h : h + HEAD]
                        if kind == 0:
                            q_s[pl.ds(row0, n), n0 + h : n0 + h + HEAD] = turn(v, row0, n, qf)
                        elif kind == 1:
                            kv[pl.ds(row0 + SIDE, n), n0 + h : n0 + h + HEAD] = turn(v, row0, n, 1.0)
                        else:
                            kv[pl.ds(row0 + SIDE, n), kc + n0 + h : kc + n0 + h + HEAD] = v.astype(BF16)
                    off += n

    lat2 = latb.reshape(ntp * rows, width)
    own.wait_recv()
    base = pl.multiple_of(x * CORES * rows, CORES * rows)
    normed(lat2, base, mb, 0, CORES * rows, 0, 2)
    project([(base, CORES * rows)])

    left = at_sp(lax.rem(sp + nsp - 1, nsp))
    right = at_sp(lax.rem(sp + 1, nsp))
    to_left = remote(kv.at[pl.ds(SIDE, SIDE)], kv.at[pl.ds(SIDE + tokens, SIDE)], hsend.at[0], hrecv.at[0], left)
    to_right = remote(kv.at[pl.ds(tokens, SIDE)], kv.at[pl.ds(0, SIDE)], hsend.at[1], hrecv.at[1], right)

    @pl.when(x == 0)
    def _():
        to_left.start()

    @pl.when(x == nx - 1)
    def _():
        to_right.start()

    for d in range(1, nx):
        for j in range(CUTS):
            if j > 0:
                lat_copy(d, j).wait_recv()
                fwd_copy(d, j).start()
            r_a = pl.multiple_of((from_x(d) * CORES + c) * rows + j * cut, cut)
            r_b = pl.multiple_of((from_x(d) * CORES + oc) * rows + j * cut, cut)
            normed(lat2, r_a, mb, 0, cut, 0, 2)
            fwd_copy(d, j).wait_recv()
            normed(lat2, r_b, mb, cut, cut, 0, 2)
            project([(r_a, cut), (r_b, cut)])

    @pl.when(x != 0)
    def _():
        to_left.start()

    @pl.when(x != nx - 1)
    def _():
        to_right.start()

    for cp in ccopies:
        cp.wait_recv()
    loads[8].wait()

    band = rows + 2 * SIDE
    key_i = lax.broadcasted_iota(jnp.int32, (rows, band), 1)
    gap = key_i - lax.broadcasted_iota(jnp.int32, (rows, band), 0)
    near = (gap >= 0) & (gap <= 2 * SIDE)

    def attend(t):
        r0 = pl.multiple_of(t * rows, rows)
        kpos = key_i + (sp * tokens + r0 - SIDE)
        valid = near & (kpos >= 0) & (kpos < tokens * nsp)
        bias = jnp.where(valid, 0.0, MASKED)
        bias = jnp.concatenate([bias] * group, axis=0)
        for h in range(kv_heads):
            heads = [h * group + i for i in range(group)]
            q = jnp.concatenate([q_s[pl.ds(r0, rows), j * HEAD : (j + 1) * HEAD] for j in heads], axis=0)
            kb = kv[pl.ds(r0, band), h * HEAD : (h + 1) * HEAD]
            vb = kv[pl.ds(r0, band), kc + h * HEAD : kc + (h + 1) * HEAD]
            kx = ctxkv[:, h * HEAD : (h + 1) * HEAD]
            vx = ctxkv[:, kc + h * HEAD : kc + (h + 1) * HEAD]
            dims = (((1,), (1,)), ((), ()))
            sb = lax.dot_general(q, kb, dims, preferred_element_type=F32) + bias
            sx = lax.dot_general(q, kx, dims, preferred_element_type=F32)
            snk = jnp.concatenate(
                [jnp.broadcast_to(sink[pl.ds(tp * (qc // HEAD) + j, 1), 0:1], (rows, 1)) for j in heads], axis=0
            ) * LOG2E
            top = jnp.maximum(
                jnp.maximum(jnp.max(sb, axis=-1, keepdims=True), jnp.max(sx, axis=-1, keepdims=True)), snk
            )
            eb = jnp.exp2(sb - top)
            ex = jnp.exp2(sx - top)
            den = jnp.sum(eb, axis=-1, keepdims=True) + jnp.sum(ex, axis=-1, keepdims=True) + jnp.exp2(snk - top)
            o = jnp.dot(eb.astype(BF16), vb, preferred_element_type=F32) + jnp.dot(
                ex.astype(BF16), vx, preferred_element_type=F32
            )
            o = (o / den).astype(BF16)
            for i, j in enumerate(heads):
                att[:, j * HEAD : (j + 1) * HEAD] = o[i * rows : (i + 1) * rows]

    piece_rows = rows // PIECES
    ntile = min(512, width)

    def x_copy(g, p, xo):
        return remote(
            comb.at[g, pl.ds(p * piece_rows, piece_rows)], xrcv.at[g, pl.ds(p * piece_rows, piece_rows)],
            xsend.at[g, p], xrecv.at[g, p], at_tp(xo * CORES + c),
        )

    def d_copy(g):
        return remote(stage.at[g, 0], prcv.at[g], dsend.at[g], drecv.at[g], partner)

    for g in range(nx):
        xo = lax.rem(x + 1 + g, nx)
        if g == 0:
            @pl.when(x != 0)
            def _():
                to_right.wait_recv()

            @pl.when(x != nx - 1)
            def _():
                to_left.wait_recv()
        if g == nx - 1:
            @pl.when(x == 0)
            def _():
                to_right.wait_recv()

            @pl.when(x == nx - 1)
            def _():
                to_left.wait_recv()

        @pl.loop(0, 2)
        def _(u):
            attend(xo * CORES + lax.rem(oc + u, 2))

            @pl.loop(0, width // ntile)
            def _(n):
                cs = pl.ds(pl.multiple_of(n * ntile, ntile), ntile)
                stage[g, u, :, cs] = jnp.dot(att[...], wo[:, cs], preferred_element_type=F32).astype(BF16)

            @pl.when(u == 0)
            def _():
                d_copy(g).start()

        d_copy(g).wait_recv()
        if g < nx - 1:
            for p in range(PIECES):
                sl = slice(p * piece_rows, (p + 1) * piece_rows)
                comb[g, sl, :] = (stage[g, 1, sl, :].astype(F32) + prcv[g, sl, :].astype(F32)).astype(BF16)
                x_copy(g, p, xo).start()

    last = nx - 1
    for p in range(PIECES):
        sl = slice(p * piece_rows, (p + 1) * piece_rows)
        total = stage[last, 1, sl, :].astype(F32) + prcv[last, sl, :].astype(F32)
        for g in range(nx - 1):
            x_copy(g, p, lax.rem(x + 1 + g, nx)).wait_recv()
            total = total + xrcv[g, sl, :].astype(F32)
        base_rows = latb[tp, sl, :].astype(F32)
        out[sl, :] = (base_rows + mod[4:5, :] * total).astype(BF16)

    for cp in mcopies + tcopies + ccopies + [own, to_left, to_right]:
        cp.wait_send()
    for d in range(1, nx):
        for j in range(CUTS):
            lat_copy(d, j).wait_send()
            fwd_copy(d, j).wait_send()
    for g in range(nx):
        d_copy(g).wait_send()
        if g < nx - 1:
            for p in range(PIECES):
                x_copy(g, p, lax.rem(x + 1 + g, nx)).wait_send()


def shards(lat, ctx, cond, ctx_cond, w_shift, w_scale, w_gate, w_q, w_k, w_v, w_o, sink):
    nsp = lax.axis_size("sp")
    ntp = lax.axis_size("tp")
    nx = ntp // CORES
    rows, width = lat.shape
    crows = ctx.shape[0]
    tokens = rows * ntp
    qc = w_q.shape[1]
    kc = w_k.shape[1]
    mrows, mcols = w_shift.shape
    half = HEAD // 2
    lane = jnp.arange(HEAD)
    inverse = THETA ** (-(lane % (half // 2)).astype(F32) * 2.0 / half)
    pos = lax.axis_index("sp") * tokens + jnp.arange(tokens, dtype=jnp.int32)[:, None]
    spot = jnp.where(lane[None, :] < half, pos // GRID_WIDTH, pos % GRID_WIDTH).astype(F32)
    angle = spot * inverse[None, :]
    cos_t = jnp.cos(angle)
    sin_t = jnp.sin(angle) * jnp.where(lane % half < half // 2, -1.0, 1.0)[None, :]
    sink_b = jnp.broadcast_to(sink[:, None], (sink.shape[0], 128))

    any_ = pl.BlockSpec(memory_space=pl.ANY)
    vmem = pl.BlockSpec(memory_space=pltpu.VMEM)
    dma = pltpu.SemaphoreType.DMA
    V = pltpu.VMEM
    return pl.pallas_call(
        functools.partial(body, nsp, ntp),
        out_shape=jax.ShapeDtypeStruct((rows, width), BF16),
        in_specs=[any_, any_, vmem, vmem] + [any_] * 7 + [vmem] * 3,
        out_specs=vmem,
        scratch_shapes=[
            V((3, mrows, mcols), BF16), V((width, qc), BF16), V((width, kc), BF16), V((width, kc), BF16),
            V((qc, width), BF16), V((ntp, rows, width), BF16), V((crows, width), BF16),
            V((max(CORES * rows, crows), width), BF16), V((8, mcols), F32), V((nsp - 1, 8, mcols), F32),
            V((8, mcols), F32), V((8, width), F32), V((nsp * crows, 2 * kc), BF16), V((tokens, qc), BF16),
            V((tokens + 2 * SIDE, 2 * kc), BF16), V((rows, qc), BF16),
            V((nx, 2, rows, width), BF16), V((nx, rows, width), BF16),
            V((nx - 1, rows, width), BF16), V((nx - 1, rows, width), BF16),
            dma((9,)), dma((nsp - 1,)), dma((nsp - 1,)), dma((ntp - 1,)), dma((ntp - 1,)),
            dma((nx - 1, CUTS)), dma((nx - 1, CUTS)), dma((nx - 1, CUTS)), dma((nx - 1, CUTS)), dma, dma,
            dma((nsp - 1,)), dma((nsp - 1,)), dma((2,)), dma((2,)), dma((nx,)), dma((nx,)),
            dma((nx - 1, PIECES)), dma((nx - 1, PIECES)),
        ],
        compiler_params=pltpu.CompilerParams(
            collective_id=0, has_side_effects=True, vmem_limit_bytes=60 * 1024 * 1024
        ),
    )(
        lat, ctx, cond.reshape(nsp, mrows), ctx_cond.reshape(nsp, mrows),
        w_shift, w_scale, w_gate, w_q, w_k, w_v, w_o, sink_b, cos_t, sin_t,
    )


def solution(mesh):
    in_specs = (
        P(("sp", "tp"), None), P("sp", None), P(), P(), P("sp", "tp"), P("sp", "tp"), P("sp", "tp"),
        P(None, "tp"), P(None, "tp"), P(None, "tp"), P("tp", None), P(),
    )
    return jax.shard_map(
        shards, mesh=mesh, in_specs=in_specs, out_specs=P(("sp", "tp"), None), check_vma=False
    )
```

time: 260 us -> 91.4 us (0.35); the launches traced: 256 us -> 91.1 us
  waiting for transfers between devices: 104 us -> 0 us
  Pallas kernels: 0 us -> 83 us
  blocking collectives: 45.8 us -> 0 us
  matrix products: 36.1 us -> 0 us
  other arithmetic: 28.1 us -> 1.85 us
  local copies, waits for them, and re-layouts: 22.1 us -> 6.25 us
  between operations: 13.6 us -> 0.02 us
  starting transfers between devices: 6.46 us -> 0 us
    pallas_call x0 -> x1, Pallas kernels: none -> 83 us  [shards(): pl.pallas_call(functools.partial(body, nsp, ntp), out_shape=jax.ShapeDtyp...]
    all_gather x2 -> x0, waiting for transfers between devices: 64.4 us -> none  [the longest x1 34.8 us: shards(): lax.all_gather(jnp.concatenate([jnp.dot(ctx_mod, key_weight, preferred_el...]
    reduce_scatter x1 -> x0, waiting for transfers between devices: 39.7 us -> none  [shards(): lax.psum_scatter(jnp.dot(attended, w_out, preferred_element_type=jnp.floa...]
    dot_general x13 -> x0, matrix products: 36.1 us -> none  [the longest x1 6.47 us: shards(): jnp.dot(attended, w_out, preferred_element_type=jnp.float32)]
    psum x1 -> x0, blocking collectives: 30.1 us -> none  [shards(): lax.psum((shift_part, scale_part, gate_part), 'sp')]
    all_gather x3 -> x0, blocking collectives: 15.7 us -> none  [the longest x1 5.34 us: shards(): lax.all_gather(gate_sum, 'tp', axis=1, tiled=True)]
    convert_element_type x7 -> x0, other arithmetic: 11.3 us -> none  [the longest x1 4.64 us: sink_weights(): (expo / (jnp.sum(expo, axis=-1, keepdims=True) + jnp.exp(sink_column - to...]
    concatenate x8 -> x0, local copies, waits for them, and re-layouts: 7.91 us -> none  [axial_rotation(): jnp.concatenate([rotate_half(values[..., :width], token_position // grid,...]
  transfers between devices with their start and end apart: 5 -> 0, of which waited for: 4 -> 0; matrix products, arithmetic and copies ran while one was open for 7% -> 0% of each run, Pallas kernels for 0% -> 0%
where the time goes in v1:
time: 91.4 us; the launch traced here: 91.1 us
  Pallas kernels  83 us (91%)
  local copies, waits for them, and re-layouts  6.25 us (7%)
  other arithmetic  1.85 us (2%)
    pallas_call x1, Pallas kernels, shards(): pl.pallas_call(functools.partial(body, nsp, ntp), out_shape=jax.ShapeDtyp...  83 us
    unnamed x1, local copies, waits for them, and re-layouts  2.29 us

profile of v1, /device:TPU:14, one launch (start us, length us, event | category | flops | bytes accessed | tf_op | source)
XLA Modules:
  0.0 91.1 jit_solution(4900716012151839469)
XLA Ops:
  0.0 1.3 %broadcast_in_dim.42.sink = f32[16,128]{1,0:T(8,128)} broadcast(f32[16]{0:T(128)} %param.23), dimensions={0} | broadcast | bytes 8256 | tf_op jit(solution)/shard_map/broadcast_in_dim | solution.py:372
  1.4 1.3 %reshape.92.cond = f32[8,512]{1,0:T(8,128)} reshape(f32[4096]{0:T(1024)} %param.14) | data formatting | bytes 32768 | tf_op jit(solution)/shard_map/reshape | solution.py:400
  2.7 1.3 %reshape.93.ctx_cond = f32[8,512]{1,0:T(8,128)} reshape(f32[4096]{0:T(1024)} %param.15) | data formatting | bytes 32768 | tf_op jit(solution)/shard_map/reshape | solution.py:400
  4.0 1.8 %sine_multiply_fusion = (f32[512,128]{1,0:T(8,128)}, f32[512,128]{1,0:T(8,128)}) fusion(f32[128]{0:T(128)S(1)} %get-tuple-element.9, f32[128]{0:T(128)S(1)} %get-tuple-element.10, s32[512]{0:T(512)S(1)} %get-tuple-element.7, s32[512]{0:T(512)S(1)} %get-tuple-element.8, pred[128]{0:T(512)(128)(4,1)S(1)} %iota_compare_fusion), kind=kLoop, calls=%fused_computation | loop fusion | flops 262144 | bytes 529536 | tf_op jit(solution)/shard_map/mul | solution.py:371
  5.8 83.0 %shard_map.118 = bf16[128,4096]{1,0:T(8,128)(2,1)} custom-call(bf16[128,4096]{1,0:T(8,128)(2,1)} %lat.1, bf16[128,4096]{1,0:T(8,128)(2,1)} %ctx.1, f32[8,512]{1,0:T(8,128)} %reshape.92.cond, f32[8,512]{1,0:T(8,128)} %reshape.93.ctx_cond, bf16[512,1024]{1,0:T(8,128)(2,1)} %w_shift.1, bf16[512,1024]{1,0:T(8,128)(2,1)} %w_scale.1, bf16[512,1024]{1,0:T(8,128)(2,1)} %w_gate.1, ...), custom_call_target="tpu_custom_call" | custom-call | tf_op jit(solution)/shard_map/pallas_call | solution.py:378
  88.8 2.3 %copy.14 = bf16[128,4096]{1,0:T(8,128)(2,1)} copy(bf16[128,4096]{1,0:T(8,128)(2,1)} %shard_map.118) | data formatting | bytes 2097152
  (3 shorter events, 0.0 us)

commit v2 on v1

--- a/solution.py
+++ b/solution.py
@@ -19,15 +19,16 @@
 F32 = jnp.float32
 BF16 = jnp.bfloat16
 CUTS = 2
-PIECES = 4
+TILES = 4
 CORES = 2
 
 
 def body(
     nsp, ntp,
-    lat, ctx, cond, ctx_cond, w_shift, w_scale, w_gate, w_q, w_k, w_v, w_o, sink, cos_t, sin_t,
+    lat, ctx, cond, ctx_cond, w_shift, w_scale, w_gate, w_q, w_k, w_v, w_o, sink,
     out,
-    wmod, wq, wk, wv, wo, latb, ctxb, mb, part, mgath, tot, mod, ctxkv, q_s, kv, att,
+    cos_t, sin_t, st_mean, st_rstd, tslots,
+    wmod, wq, wk, wv, wo, latb, ctxb, mb, part, mgath, mod, ctxkv, q_s, kv, att,
     stage, prcv, comb, xrcv,
     load_sem, msend, mrecv, tsend, trecv, lsend, lrecv, fsend, frecv, psend, precv,
     csend, crecv, hsend, hrecv, dsend, drecv, xsend, xrecv,
@@ -71,7 +72,7 @@
             ]
         )
     ]
-    for load in loads:
+    for load in loads[:3]:
         load.start()
 
     barrier = pltpu.get_barrier_semaphore()
@@ -100,9 +101,12 @@
     own = remote(lat, latb.at[tp], psend, precv, partner)
     own.start()
 
-    a0 = jax.nn.silu(cond[pl.ds(sp, 1), :]).astype(BF16).astype(F32)
-    a1 = jax.nn.silu(ctx_cond[pl.ds(sp, 1), :]).astype(BF16).astype(F32)
+    mrows = w_shift.shape[0]
+    arow = pl.ds(pl.multiple_of(sp * mrows, mrows), mrows)
+    a0 = jax.nn.silu(cond[arow].reshape(1, mrows)).astype(BF16).astype(F32)
+    a1 = jax.nn.silu(ctx_cond[arow].reshape(1, mrows)).astype(BF16).astype(F32)
     line = lax.broadcasted_iota(jnp.int32, (8, a0.shape[1]), 0)
+    line8 = lax.broadcasted_iota(jnp.int32, (8, mcols // 2), 0)
     z = jnp.zeros((8, a0.shape[1]), F32)
     a0 = jnp.broadcast_to(a0, z.shape)
     a1 = jnp.broadcast_to(a1, z.shape)
@@ -112,23 +116,60 @@
         loads[i].wait()
         piece = jnp.dot(act, wmod[i], preferred_element_type=F32)
         acc = piece if acc is None else acc + piece
-    part[...] = acc
+    hc = mcols // 2
+    part[...] = jnp.concatenate([acc[:, :hc], acc[:, hc:]], axis=0).astype(BF16)
     mcopies = [
         remote(part, mgath.at[d - 1], msend.at[d - 1], mrecv.at[d - 1], at_sp(lax.rem(sp + d, nsp)))
         for d in range(1, nsp)
     ]
     for cp in mcopies:
         cp.start()
-    for i in range(3, 8):
-        loads[i].wait()
-    acc = part[...]
+    for i in (3, 7, 4, 5, 6, 8):
+        loads[i].start()
+
+    def turn_tables():
+        half = HEAD // 2
+        lane_i = lax.broadcasted_iota(jnp.int32, (tokens, HEAD), 1)
+        inner = lax.rem(lane_i, half // 2).astype(F32)
+        inverse = jnp.exp(inner * (-2.0 / half * math.log(THETA)))
+        pos = (lax.broadcasted_iota(jnp.int32, (tokens, HEAD), 0) + sp * tokens).astype(F32)
+        grid_row = jnp.floor(pos * (1.0 / GRID_WIDTH))
+        angle = jnp.where(lane_i < half, grid_row, pos - grid_row * GRID_WIDTH) * inverse
+        cos_t[...] = jnp.cos(angle)
+        sin_t[...] = jnp.where(lax.rem(lane_i, half) < half // 2, -1.0, 1.0) * jnp.sin(angle)
+
+    step = 16
+
+    def measure_rows(src, row0, st0, count):
+        @pl.loop(0, count // step)
+        def _(i):
+            v = src[pl.ds(row0 + i * step, step), :].astype(F32)
+            mean = jnp.mean(v, axis=-1, keepdims=True)
+            v = v - mean
+            var = jnp.mean(v * v, axis=-1, keepdims=True)
+            st_mean[pl.ds(st0 + i * step, step), :] = jnp.broadcast_to(mean, (step, HEAD))
+            st_rstd[pl.ds(st0 + i * step, step), :] = jnp.broadcast_to(lax.rsqrt(var + EPS), (step, HEAD))
+
+    def shift_rows(src, row0, st0, dst, dst0, count, r_shift, r_scale):
+        @pl.loop(0, count // step)
+        def _(i):
+            v = src[pl.ds(row0 + i * step, step), :].astype(F32)
+            srow = pl.ds(st0 + i * step, step)
+            v = (v - st_mean[srow, 0:1]) * st_rstd[srow, 0:1]
+            v = v * mod[r_scale : r_scale + 1, :] + mod[r_shift : r_shift + 1, :]
+            dst[pl.ds(dst0 + i * step, step), :] = v.astype(BF16)
+
+    lat2 = latb.reshape(ntp * rows, width)
+    base = pl.multiple_of(x * CORES * rows, CORES * rows)
+    loads[3].wait()
+    measure_rows(ctxb, 0, 0, crows)
+    acc = part[...].astype(F32)
     for d in range(1, nsp):
         mcopies[d - 1].wait_recv()
-        acc = acc + mgath[d - 1]
-    tot[...] = acc
-    mine = pl.ds(pl.multiple_of(tp * mcols, mcols), mcols)
+        acc = acc + mgath[d - 1].astype(F32)
+    tslots[tp] = acc.astype(BF16)
     tcopies = [
-        remote(tot, mod.at[:, mine], tsend.at[d - 1], trecv.at[d - 1], at_tp(lax.rem(tp + d, ntp)))
+        remote(tslots.at[tp], tslots.at[tp], tsend.at[d - 1], trecv.at[d - 1], at_tp(lax.rem(tp + d, ntp)))
         for d in range(1, ntp)
     ]
     for cp in tcopies:
@@ -136,24 +177,18 @@
     for d in range(1, nx):
         for j in range(1, CUTS):
             lat_copy(d, j).start()
-    mod[:, mine] = acc
+    turn_tables()
     for cp in tcopies:
         cp.wait_recv()
-
-    def normed(src, row0, dst, dst0, count, r_shift, r_scale):
-        step = 16
-
-        @pl.loop(0, count // step)
-        def _(i):
-            v = src[pl.ds(row0 + i * step, step), :].astype(F32)
-            mean = jnp.mean(v, axis=-1, keepdims=True)
-            v = v - mean
-            var = jnp.mean(v * v, axis=-1, keepdims=True)
-            v = v * lax.rsqrt(var + EPS)
-            v = v * (1.0 + mod[r_scale : r_scale + 1, :]) + mod[r_shift : r_shift + 1, :]
-            dst[pl.ds(dst0 + i * step, step), :] = v.astype(BF16)
-
-    normed(ctxb, 0, mb, 0, crows, 1, 3)
+    for t in range(ntp):
+        v = tslots[t].astype(F32)
+        bump = jnp.where((line8 == 2) | (line8 == 3), 1.0, 0.0)
+        mod[:, t * mcols : t * mcols + hc] = v[0:8] + bump
+        mod[:, t * mcols + hc : (t + 1) * mcols] = v[8:16] + bump
+    loads[4].wait()
+    loads[5].wait()
+
+    shift_rows(ctxb, 0, 0, mb, 0, crows, 1, 3)
     crow = pl.ds(pl.multiple_of(sp * crows, crows), crows)
     cm = mb[0:crows, :]
     ctxkv[crow, 0:kc] = jnp.dot(cm, wk[...], preferred_element_type=F32).astype(BF16)
@@ -197,10 +232,11 @@
                             kv[pl.ds(row0 + SIDE, n), kc + n0 + h : kc + n0 + h + HEAD] = v.astype(BF16)
                     off += n
 
-    lat2 = latb.reshape(ntp * rows, width)
+    loads[6].wait()
+    loads[7].wait()
     own.wait_recv()
-    base = pl.multiple_of(x * CORES * rows, CORES * rows)
-    normed(lat2, base, mb, 0, CORES * rows, 0, 2)
+    measure_rows(lat2, base, 0, CORES * rows)
+    shift_rows(lat2, base, 0, mb, 0, CORES * rows, 0, 2)
     project([(base, CORES * rows)])
 
     left = at_sp(lax.rem(sp + nsp - 1, nsp))
@@ -223,9 +259,11 @@
                 fwd_copy(d, j).start()
             r_a = pl.multiple_of((from_x(d) * CORES + c) * rows + j * cut, cut)
             r_b = pl.multiple_of((from_x(d) * CORES + oc) * rows + j * cut, cut)
-            normed(lat2, r_a, mb, 0, cut, 0, 2)
+            measure_rows(lat2, r_a, 0, cut)
+            shift_rows(lat2, r_a, 0, mb, 0, cut, 0, 2)
             fwd_copy(d, j).wait_recv()
-            normed(lat2, r_b, mb, cut, cut, 0, 2)
+            measure_rows(lat2, r_b, cut, cut)
+            shift_rows(lat2, r_b, cut, mb, cut, cut, 0, 2)
             project([(r_a, cut), (r_b, cut)])
 
     @pl.when(x != 0)
@@ -245,7 +283,7 @@
     gap = key_i - lax.broadcasted_iota(jnp.int32, (rows, band), 0)
     near = (gap >= 0) & (gap <= 2 * SIDE)
 
-    def attend(t):
+    def attend(t, u):
         r0 = pl.multiple_of(t * rows, rows)
         kpos = key_i + (sp * tokens + r0 - SIDE)
         valid = near & (kpos >= 0) & (kpos < tokens * nsp)
@@ -262,7 +300,7 @@
             sb = lax.dot_general(q, kb, dims, preferred_element_type=F32) + bias
             sx = lax.dot_general(q, kx, dims, preferred_element_type=F32)
             snk = jnp.concatenate(
-                [jnp.broadcast_to(sink[pl.ds(tp * (qc // HEAD) + j, 1), 0:1], (rows, 1)) for j in heads], axis=0
+                [jnp.full((rows, 1), sink[tp * (qc // HEAD) + j], F32) for j in heads], axis=0
             ) * LOG2E
             top = jnp.maximum(
                 jnp.maximum(jnp.max(sb, axis=-1, keepdims=True), jnp.max(sx, axis=-1, keepdims=True)), snk
@@ -275,19 +313,27 @@
             )
             o = (o / den).astype(BF16)
             for i, j in enumerate(heads):
-                att[:, j * HEAD : (j + 1) * HEAD] = o[i * rows : (i + 1) * rows]
-
-    piece_rows = rows // PIECES
-    ntile = min(512, width)
-
-    def x_copy(g, p, xo):
+                att[u, :, j * HEAD : (j + 1) * HEAD] = o[i * rows : (i + 1) * rows]
+
+    tile_cols = width // TILES
+    ntile = min(512, tile_cols)
+
+    def cols_of(n):
+        return slice(n * tile_cols, (n + 1) * tile_cols)
+
+    def x_copy(g, n, xo):
         return remote(
-            comb.at[g, pl.ds(p * piece_rows, piece_rows)], xrcv.at[g, pl.ds(p * piece_rows, piece_rows)],
-            xsend.at[g, p], xrecv.at[g, p], at_tp(xo * CORES + c),
+            comb.at[g, n], xrcv.at[g, n], xsend.at[g, n], xrecv.at[g, n], at_tp(xo * CORES + c)
         )
 
-    def d_copy(g):
-        return remote(stage.at[g, 0], prcv.at[g], dsend.at[g], drecv.at[g], partner)
+    def d_copy(g, n):
+        return remote(stage.at[g, 0, n], prcv.at[g, n], dsend.at[g, n], drecv.at[g, n], partner)
+
+    def combine(g, n, xo):
+        d_copy(g, n).wait_recv()
+        if g < nx - 1:
+            comb[g, n] = (stage[g, 1, n].astype(F32) + prcv[g, n].astype(F32)).astype(BF16)
+            x_copy(g, n, xo).start()
 
     for g in range(nx):
         xo = lax.rem(x + 1 + g, nx)
@@ -310,33 +356,27 @@
 
         @pl.loop(0, 2)
         def _(u):
-            attend(xo * CORES + lax.rem(oc + u, 2))
-
-            @pl.loop(0, width // ntile)
-            def _(n):
-                cs = pl.ds(pl.multiple_of(n * ntile, ntile), ntile)
-                stage[g, u, :, cs] = jnp.dot(att[...], wo[:, cs], preferred_element_type=F32).astype(BF16)
-
-            @pl.when(u == 0)
-            def _():
-                d_copy(g).start()
-
-        d_copy(g).wait_recv()
-        if g < nx - 1:
-            for p in range(PIECES):
-                sl = slice(p * piece_rows, (p + 1) * piece_rows)
-                comb[g, sl, :] = (stage[g, 1, sl, :].astype(F32) + prcv[g, sl, :].astype(F32)).astype(BF16)
-                x_copy(g, p, xo).start()
+            attend(xo * CORES + lax.rem(oc + u, 2), u)
+
+        for n in range(TILES):
+            for u in range(2):
+                for k in range(0, tile_cols, ntile):
+                    stage[g, u, n, :, k : k + ntile] = jnp.dot(
+                        att[u], wo[:, n * tile_cols + k : n * tile_cols + k + ntile], preferred_element_type=F32
+                    ).astype(BF16)
+                if u == 0:
+                    d_copy(g, n).start()
+            if n > 0:
+                combine(g, n - 1, xo)
+        combine(g, TILES - 1, xo)
 
     last = nx - 1
-    for p in range(PIECES):
-        sl = slice(p * piece_rows, (p + 1) * piece_rows)
-        total = stage[last, 1, sl, :].astype(F32) + prcv[last, sl, :].astype(F32)
+    for n in range(TILES):
+        total = stage[last, 1, n].astype(F32) + prcv[last, n].astype(F32)
         for g in range(nx - 1):
-            x_copy(g, p, lax.rem(x + 1 + g, nx)).wait_recv()
-            total = total + xrcv[g, sl, :].astype(F32)
-        base_rows = latb[tp, sl, :].astype(F32)
-        out[sl, :] = (base_rows + mod[4:5, :] * total).astype(BF16)
+            x_copy(g, n, lax.rem(x + 1 + g, nx)).wait_recv()
+            total = total + xrcv[g, n].astype(F32)
+        out[:, cols_of(n)] = (latb[tp, :, cols_of(n)].astype(F32) + mod[4:5, cols_of(n)] * total).astype(BF16)
 
     for cp in mcopies + tcopies + ccopies + [own, to_left, to_right]:
         cp.wait_send()
@@ -345,10 +385,10 @@
             lat_copy(d, j).wait_send()
             fwd_copy(d, j).wait_send()
     for g in range(nx):
-        d_copy(g).wait_send()
-        if g < nx - 1:
-            for p in range(PIECES):
-                x_copy(g, p, lax.rem(x + 1 + g, nx)).wait_send()
+        for n in range(TILES):
+            d_copy(g, n).wait_send()
+            if g < nx - 1:
+                x_copy(g, n, lax.rem(x + 1 + g, nx)).wait_send()
 
 
 def shards(lat, ctx, cond, ctx_cond, w_shift, w_scale, w_gate, w_q, w_k, w_v, w_o, sink):
@@ -361,16 +401,6 @@
     qc = w_q.shape[1]
     kc = w_k.shape[1]
     mrows, mcols = w_shift.shape
-    half = HEAD // 2
-    lane = jnp.arange(HEAD)
-    inverse = THETA ** (-(lane % (half // 2)).astype(F32) * 2.0 / half)
-    pos = lax.axis_index("sp") * tokens + jnp.arange(tokens, dtype=jnp.int32)[:, None]
-    spot = jnp.where(lane[None, :] < half, pos // GRID_WIDTH, pos % GRID_WIDTH).astype(F32)
-    angle = spot * inverse[None, :]
-    cos_t = jnp.cos(angle)
-    sin_t = jnp.sin(angle) * jnp.where(lane % half < half // 2, -1.0, 1.0)[None, :]
-    sink_b = jnp.broadcast_to(sink[:, None], (sink.shape[0], 128))
-
     any_ = pl.BlockSpec(memory_space=pl.ANY)
     vmem = pl.BlockSpec(memory_space=pltpu.VMEM)
     dma = pltpu.SemaphoreType.DMA
@@ -378,27 +408,29 @@
     return pl.pallas_call(
         functools.partial(body, nsp, ntp),
         out_shape=jax.ShapeDtypeStruct((rows, width), BF16),
-        in_specs=[any_, any_, vmem, vmem] + [any_] * 7 + [vmem] * 3,
+        in_specs=[any_, any_, vmem, vmem] + [any_] * 7 + [pl.BlockSpec(memory_space=pltpu.SMEM)],
         out_specs=vmem,
         scratch_shapes=[
+            V((tokens, HEAD), F32), V((tokens, HEAD), F32), V((max(CORES * rows, crows), HEAD), F32),
+            V((max(CORES * rows, crows), HEAD), F32), V((ntp, 16, mcols // 2), BF16),
             V((3, mrows, mcols), BF16), V((width, qc), BF16), V((width, kc), BF16), V((width, kc), BF16),
             V((qc, width), BF16), V((ntp, rows, width), BF16), V((crows, width), BF16),
-            V((max(CORES * rows, crows), width), BF16), V((8, mcols), F32), V((nsp - 1, 8, mcols), F32),
-            V((8, mcols), F32), V((8, width), F32), V((nsp * crows, 2 * kc), BF16), V((tokens, qc), BF16),
-            V((tokens + 2 * SIDE, 2 * kc), BF16), V((rows, qc), BF16),
-            V((nx, 2, rows, width), BF16), V((nx, rows, width), BF16),
-            V((nx - 1, rows, width), BF16), V((nx - 1, rows, width), BF16),
+            V((max(CORES * rows, crows), width), BF16), V((16, mcols // 2), BF16), V((nsp - 1, 16, mcols // 2), BF16),
+            V((8, width), F32), V((nsp * crows, 2 * kc), BF16), V((tokens, qc), BF16),
+            V((tokens + 2 * SIDE, 2 * kc), BF16), V((2, rows, qc), BF16),
+            V((nx, 2, TILES, rows, width // TILES), BF16), V((nx, TILES, rows, width // TILES), BF16),
+            V((nx - 1, TILES, rows, width // TILES), BF16), V((nx - 1, TILES, rows, width // TILES), BF16),
             dma((9,)), dma((nsp - 1,)), dma((nsp - 1,)), dma((ntp - 1,)), dma((ntp - 1,)),
             dma((nx - 1, CUTS)), dma((nx - 1, CUTS)), dma((nx - 1, CUTS)), dma((nx - 1, CUTS)), dma, dma,
-            dma((nsp - 1,)), dma((nsp - 1,)), dma((2,)), dma((2,)), dma((nx,)), dma((nx,)),
-            dma((nx - 1, PIECES)), dma((nx - 1, PIECES)),
+            dma((nsp - 1,)), dma((nsp - 1,)), dma((2,)), dma((2,)), dma((nx, TILES)), dma((nx, TILES)),
+            dma((nx - 1, TILES)), dma((nx - 1, TILES)),
         ],
         compiler_params=pltpu.CompilerParams(
             collective_id=0, has_side_effects=True, vmem_limit_bytes=60 * 1024 * 1024
         ),
     )(
-        lat, ctx, cond.reshape(nsp, mrows), ctx_cond.reshape(nsp, mrows),
-        w_shift, w_scale, w_gate, w_q, w_k, w_v, w_o, sink_b, cos_t, sin_t,
+        lat, ctx, cond, ctx_cond,
+        w_shift, w_scale, w_gate, w_q, w_k, w_v, w_o, sink,
     )
 
 

time: 91.4 us -> 81.9 us (0.90)
  local copies, waits for them, and re-layouts: 6.25 us -> 2.29 us
  Pallas kernels: 83 us -> 79.2 us
  other arithmetic: 1.85 us -> 0 us
    pallas_call x1, Pallas kernels: 83 us -> 79.2 us  [shards(): pl.pallas_call(functools.partial(body, nsp, ntp), out_shape=jax.ShapeDtyp...]
    reshape x2 -> x0, local copies, waits for them, and re-layouts: 2.64 us -> none  [the longest x1 1.32 us: shards(): cond.reshape(nsp, mrows)]
    mul x1 -> x0, other arithmetic: 1.82 us -> none  [shards(): jnp.sin(angle) * jnp.where(lane % half < half // 2, -1.0, 1.0)[None, :]]
    broadcast_in_dim x1 -> x0, local copies, waits for them, and re-layouts: 1.32 us -> none  [shards(): sink_b = jnp.broadcast_to(sink[:, None], (sink.shape[0], 128))]
where the time goes in v2:
time: 81.9 us; the launch traced here: 81.5 us
  Pallas kernels  79.2 us (97%)
  local copies, waits for them, and re-layouts  2.29 us (3%)
    pallas_call x1, Pallas kernels, shards(): pl.pallas_call(functools.partial(body, nsp, ntp), out_shape=jax.ShapeDtyp...  79.2 us
    unnamed x1, local copies, waits for them, and re-layouts  2.29 us

profile of v2, /device:TPU:14, one launch (start us, length us, event | category | flops | bytes accessed | tf_op | source)
XLA Modules:
  0.0 81.5 jit_solution(8561362387307675705)
XLA Ops:
  0.0 79.2 %shard_map.118 = bf16[128,4096]{1,0:T(8,128)(2,1)} custom-call(bf16[128,4096]{1,0:T(8,128)(2,1)} %lat.1, bf16[128,4096]{1,0:T(8,128)(2,1)} %ctx.1, f32[4096]{0:T(1024)} %cond.1, f32[4096]{0:T(1024)} %ctx_cond.1, bf16[512,1024]{1,0:T(8,128)(2,1)} %w_shift.1, bf16[512,1024]{1,0:T(8,128)(2,1)} %w_scale.1, bf16[512,1024]{1,0:T(8,128)(2,1)} %w_gate.1, ...), custom_call_target="tpu_custom_call" | custom-call | tf_op jit(solution)/shard_map/pallas_call | solution.py:408
  79.2 2.3 %copy.14 = bf16[128,4096]{1,0:T(8,128)(2,1)} copy(bf16[128,4096]{1,0:T(8,128)(2,1)} %shard_map.118) | data formatting | bytes 2097152
